TPU v7x, 1024 devices: a whole 8x8x8 slice. The times are simulated.
1024 devices in a mesh: sp: 16 (over x, core), dp: 64 (over z, y).
Axes of the slice: x: 8, y: 8, z: 8, core: 2. Of those that a mesh axis runs over, the one named last changes fastest.
Arguments:
- queries: bfloat16 [128, 8, 2304, 128], P('dp', None, 'sp'), may hold values from -6 to 6
- keys: bfloat16 [128, 8, 2304, 128], P('dp', None, 'sp'), may hold values from -6 to 6
- values: bfloat16 [128, 8, 2304, 128], P('dp', None, 'sp'), may hold values from -6 to 6
- in_gate: bfloat16 [128, 8, 2304], P('dp', None, 'sp'), may hold values from -5 to 240
- forget_gate: bfloat16 [128, 8, 2304], P('dp', None, 'sp'), may hold values from 1 to 20
- out_gate: bfloat16 [128, 8, 2304, 128], P('dp', None, 'sp'), may hold values from -6 to 6
- norm_gain: float32 [8, 128], replicated, may hold values from 0.1 to 1.9
- out_weight: bfloat16 [1024, 2048], P(None, 'dp'), may hold values from -0.1875 to 0.1875
Outputs:
- mixed: bfloat16 [128, 2304, 2048], P('dp', 'sp')
All inputs are finite; a program needn't handle non-finite values.
Results may differ from a plain program's by a relative error of at most 0.0057.
Values may be sent and summed in bfloat16 or wider, within the bound.
A program may use at most 64 MiB of HBM per device.

v0:
```python
import functools

import jax
import jax.numpy as jnp
from jax import lax
from jax.experimental import pallas as pl
from jax.experimental.pallas import tpu as pltpu
from jax.sharding import Mesh
from jax.sharding import PartitionSpec as P

MESH = pl.DeviceIdType.MESH
F32 = jnp.float32
BF16 = jnp.bfloat16
HI = lax.Precision.HIGHEST
NT = (((1,), (1,)), ((), ()))
TN = (((0,), (0,)), ((), ()))
EPS = 1e-05
HEADS = 8
PAIRS = 16
T = 144
DH = 128
SROWS = 144
RING = 8
PARTS = ((0, 80), (80, 64))
CUTS = 4
FAR = 2


def kernel(
    q_hbm, k_hbm, v_hbm, ig_hbm, fg_hbm, og_hbm, gain_hbm, w_hbm, o_hbm,
    q_ref, k_ref, v_ref, ig_ref, fg_ref, og_ref, gain_ref, o_ref, in_sem, out_sem,
    wg, state_in, state_out, state_eff, local, peer_local, num_loc, den_loc, top, hid,
    arow, wcol, stat, peer_stat, m_in, m_out, m_eff, coef,
    one_send, one_recv, ring_send, ring_recv, core_w_send, core_w_recv,
    loc_send, loc_recv, ch_send, ch_recv, eff_send, eff_recv, small_send, small_recv,
):
    x = lax.axis_index("x")
    core = lax.axis_index("c")
    z = lax.axis_index("z")
    y = lax.axis_index("y")
    other = {"c": 1 - core}
    barrier = pltpu.get_barrier_semaphore()

    def at(axis, d):
        return {axis: lax.rem(lax.axis_index(axis) + (d + RING), RING)}

    def copy(src, dst, ss, rs, dev):
        return pltpu.make_async_remote_copy(
            src_ref=src, dst_ref=dst, send_sem=ss, recv_sem=rs, device_id=dev, device_id_type=MESH
        )

    def greet(dev):
        pl.semaphore_signal(barrier, inc=1, device_id=dev, device_id_type=MESH)

    greet(other)

    @pl.when(core == 0)
    def _():
        for axis in ("y", "z"):
            for d in range(1, RING):
                greet(at(axis, d))

    @pl.when(core == 1)
    def _():
        greet(at("x", 1))
        greet(at("x", -1))

    loads = [
        pltpu.make_async_copy(src, dst, in_sem.at[i])
        for i, (src, dst) in enumerate(
            (
                (fg_hbm, fg_ref),
                (ig_hbm, ig_ref),
                (k_hbm, k_ref),
                (v_hbm, v_ref),
                (q_hbm, q_ref),
                (og_hbm, og_ref),
                (gain_hbm, gain_ref),
            )
        )
    ]
    w_load = pltpu.make_async_copy(w_hbm, wg.at[z, y], in_sem.at[7])
    for load in loads[:2]:
        load.start()

    @pl.when(core == 0)
    def _():
        w_load.start()

    for load in loads[2:]:
        load.start()

    row_i = lax.broadcasted_iota(jnp.int32, (T, T), 0)
    col_i = lax.broadcasted_iota(jnp.int32, (T, T), 1)
    lower = (col_i <= row_i).astype(BF16)
    eye = (col_i == row_i).astype(BF16)
    loads[0].wait()
    loads[1].wait()
    logf = -jnp.log1p(jnp.exp(-fg_ref[...].astype(F32)))
    rest = logf
    sum_t = jnp.zeros((T, PAIRS), F32)
    sum_r = jnp.zeros((PAIRS, T), F32)
    for _ in range(3):
        term = rest.astype(BF16)
        rest = rest - term.astype(F32)
        sum_t = sum_t + lax.dot_general(lower, term, NT, preferred_element_type=F32)
        sum_r = sum_r + lax.dot_general(term, lower, NT, preferred_element_type=F32)
    inp = ig_ref[...].astype(F32)
    inp_t = lax.dot_general(eye, ig_ref[...], NT, preferred_element_type=F32)
    arow[...] = inp - sum_r
    a_t = inp_t - sum_t
    top_row = jnp.max(a_t, axis=0, keepdims=True)
    w_t = jnp.exp(a_t - top_row) * (DH**-0.5)
    for p in range(PAIRS):
        wcol[p] = jnp.broadcast_to(w_t[:, p : p + 1], (T, DH))
    stat[0:1, 0:PAIRS] = sum_t[T - 1 : T, :]
    stat[1:2, 0:PAIRS] = top_row

    def first(half, d):
        axis = ("y", "z")[half]
        ref = wg.at[z, y, pl.ds(16 * half, 16)]
        return copy(ref, ref, one_send.at[half, d - 1], one_recv.at[half, d - 1], at(axis, d))

    def first_in(half, d):
        axis = ("y", "z")[half]
        n = lax.rem(lax.axis_index(axis) - d + RING, RING)
        dst = wg.at[z, n, pl.ds(0, 16)] if half == 0 else wg.at[n, y, pl.ds(16, 16)]
        return copy(dst, dst, one_send.at[half, d - 1], one_recv.at[half, d - 1], at(axis, d))

    def block(half, n):
        return wg.at[n, :, pl.ds(0, 16)] if half == 0 else wg.at[:, n, pl.ds(16, 16)]

    def half_block(half, n, part):
        cut = pl.ds(4 * part, 4)
        return wg.at[n, cut, pl.ds(0, 16)] if half == 0 else wg.at[cut, n, pl.ds(16, 16)]

    def second_axis(half):
        return ("z", "y")[half]

    def shifted(half, d):
        return lax.rem(lax.axis_index(second_axis(half)) + (d + RING), RING)

    def piece(half, way, s, c):
        cut = pl.ds(c * (RING // CUTS), RING // CUTS)
        n = shifted(half, -way * s)
        return wg.at[n, cut, pl.ds(0, 16)] if half == 0 else wg.at[cut, n, pl.ds(16, 16)]

    def pieces(way, s):
        return range(CUTS) if s < 4 else (range(CUTS // 2), range(CUTS // 2, CUTS))[way < 0]

    def ring_copy(half, way, s, c):
        ref = piece(half, way, s, c)
        f, i = 2 * half + (way < 0), CUTS * s + c
        return copy(ref, ref, ring_send.at[f, i], ring_recv.at[f, i], at(second_axis(half), way))

    def ring_in(half, way, s, c):
        ref = piece(half, way, s, c)
        f, i = 2 * half + (way < 0), CUTS * (s - 1) + c
        return copy(ref, ref, ring_send.at[f, i], ring_recv.at[f, i], at(second_axis(half), way))

    def core_ref(half, slot):
        if slot == 8:
            return block(half, shifted(half, 0))
        way = (1, -1)[slot % 2]
        n = shifted(half, -way * (slot // 2 + 1))
        return block(half, n) if slot < 6 else half_block(half, n, slot - 6)

    def core_copy(half, slot):
        ref = core_ref(half, slot)
        return copy(ref, ref, core_w_send.at[half, slot], core_w_recv.at[half, slot], other)

    stat_copy = copy(stat, peer_stat, small_send.at[0], small_recv.at[0], other)
    m_right = copy(m_out, m_in, small_send.at[1], small_recv.at[1], at("x", 1))
    m_core = copy(m_in, m_eff, small_send.at[2], small_recv.at[2], other)

    def loc_copy(p):
        return copy(local.at[p], peer_local.at[p], loc_send.at[p], loc_recv.at[p], other)

    def chain_copy(p, h):
        rows = pl.ds(*PARTS[h])
        return copy(
            state_out.at[p, rows], state_in.at[p, rows], ch_send.at[p, h], ch_recv.at[p, h], at("x", 1)
        )

    def eff_copy(p, h):
        rows = pl.ds(*PARTS[h])
        return copy(state_in.at[p, rows], state_eff.at[p, rows], eff_send.at[p, h], eff_recv.at[p, h], other)

    @pl.when(x == 0)
    def _():
        zero = jnp.zeros((8, DH), F32)
        m_in[...] = zero

        @pl.when(core == 0)
        def _():
            m_eff[...] = zero

        def clear(p, c):
            state_in[p] = jnp.zeros((SROWS, DH), BF16)

            @pl.when(core == 0)
            def _():
                state_eff[p] = jnp.zeros((SROWS, DH), BF16)

            return c

        lax.fori_loop(0, PAIRS, clear, 0)

    tail_i = lax.broadcasted_iota(jnp.int32, (16, DH), 0)

    def local_state(p, c):
        kw = k_ref[p].astype(F32) * wcol[p]
        n = jnp.sum(kw, axis=0, keepdims=True)
        local[p, 0:DH] = lax.dot_general(v_ref[p], kw.astype(BF16), TN, preferred_element_type=F32)
        local[p, DH:SROWS] = jnp.where(tail_i == 0, jnp.broadcast_to(n, (16, DH)), 0.0)

        return c

    loads[2].wait()
    loads[3].wait()
    lax.fori_loop(0, PAIRS, local_state, 0)

    @pl.when(core == 1)
    def _():
        pl.semaphore_wait(barrier, 3)

    @pl.when(core == 0)
    def _():
        pl.semaphore_wait(barrier, 15)
        stat_copy.start()

        def give(p, c):
            loc_copy(p).start()
            return c

        lax.fori_loop(0, PAIRS, give, 0)
        w_load.wait()
        for d in (4, 3, 5, 2, 6, 1, 7):
            first(0, d).start()
            first(1, d).start()

    for load in loads[4:]:
        load.wait()

    def attend(p, c):
        a = arow[pl.ds(p, 1), :]
        masked = jnp.where(col_i <= row_i, jnp.broadcast_to(a, (T, T)), -1e30)
        t = jnp.max(masked, axis=1, keepdims=True)
        wt = jnp.exp(masked - t) * (DH**-0.5)
        s = lax.dot_general(q_ref[p], k_ref[p], NT, preferred_element_type=F32) * wt
        den_loc[p] = jnp.broadcast_to(jnp.sum(s, axis=1, keepdims=True), (T, DH))
        top[p] = jnp.broadcast_to(t, (T, DH))
        high = s.astype(BF16)
        low = (s - high.astype(F32)).astype(BF16)
        num_loc[p] = jnp.dot(high, v_ref[p], preferred_element_type=F32) + jnp.dot(
            low, v_ref[p], preferred_element_type=F32
        )
        return c

    def attend_all():
        lax.fori_loop(0, PAIRS, attend, 0)

    def finish(p):
        t = top[p]
        m = m_eff_b(p)
        mu = jnp.maximum(t, m)
        g1 = jnp.exp(m - mu)
        g2 = jnp.exp(t - mu)
        inter = lax.dot_general(q_ref[p], state_eff[p], NT, preferred_element_type=F32)
        num = g1 * inter[:, 0:DH] + g2 * num_loc[p]
        den = g1 * jnp.broadcast_to(inter[:, DH : DH + 1], (T, DH)) + g2 * den_loc[p]
        cell = (num / jnp.maximum(jnp.abs(den), 1.0)).astype(BF16).astype(F32)
        mean = jnp.mean(cell, axis=1, keepdims=True)
        cen = cell - mean
        var = jnp.mean(cen * cen, axis=1, keepdims=True)
        h = lax.rem(p, HEADS)
        b = lax.div(p, HEADS)
        gain = gain_ref[pl.ds(h, 1), :]
        gate = 1.0 / (1.0 + jnp.exp(-og_ref[p].astype(F32)))
        out = cen * lax.rsqrt(var + EPS) * gain * gate
        hid[b, :, pl.ds(pl.multiple_of(h * DH, DH), DH)] = out.astype(BF16)

    def m_eff_b(p):
        return coef[4, pl.ds(p, 1), :]

    eye_p = lax.broadcasted_iota(jnp.int32, (PAIRS, PAIRS), 0) == lax.broadcasted_iota(
        jnp.int32, (PAIRS, PAIRS), 1
    )

    def spread(i, row):
        column = jnp.sum(jnp.where(eye_p, jnp.broadcast_to(row, (PAIRS, PAIRS)), 0.0), axis=1, keepdims=True)
        coef[i] = jnp.broadcast_to(column, (PAIRS, DH))

    def chain(p, with_finish):
        loc_copy(p).wait_recv()
        c_old, c_peer = coef[0, pl.ds(p, 1), :], coef[1, pl.ds(p, 1), :]
        c_mid, c_own = coef[2, pl.ds(p, 1), :], coef[3, pl.ds(p, 1), :]
        for h, (row, n) in enumerate(PARTS):
            rows = pl.ds(row, n)
            mid = c_peer * peer_local[p, rows]
            out = c_mid * mid + c_own * local[p, rows]

            @pl.when(x > 0)
            def _():
                chain_copy(p, h).wait_recv()
                eff_copy(p, h).start()

            old = c_old * state_in[p, rows].astype(F32)
            state_out[p, rows] = (c_mid * old + out).astype(BF16)

            @pl.when(x < RING - 1)
            def _():
                chain_copy(p, h).start()

            state_eff[p, rows] = (old + mid).astype(BF16)
        if with_finish:
            finish(p)

    def chain_all(with_finish):
        @pl.when(x > 0)
        def _():
            m_right.wait_recv()

        e0, t0 = peer_stat[0:1, 0:PAIRS], peer_stat[1:2, 0:PAIRS]
        e1, t1 = stat[0:1, 0:PAIRS], stat[1:2, 0:PAIRS]
        m0 = m_in[0:1, 0:PAIRS]
        mu0 = jnp.maximum(m0, t0)
        m1 = e0 + mu0
        mu1 = jnp.maximum(m1, t1)
        m_out[0:1, 0:PAIRS] = e1 + mu1

        @pl.when(x < RING - 1)
        def _():
            m_right.start()

        @pl.when(x > 0)
        def _():
            m_core.start()

        spread(0, jnp.exp(m0 - mu0))
        spread(1, jnp.exp(t0 - mu0))
        spread(2, jnp.exp(m1 - mu1))
        spread(3, jnp.exp(t1 - mu1))
        spread(4, m1)

        def step(p, c):
            chain(p, with_finish)
            return c

        lax.fori_loop(0, PAIRS, step, 0)

    def finish_all():
        def step(p, c):
            finish(p)
            return c

        lax.fori_loop(0, PAIRS, step, 0)

    @pl.when(core == 1)
    def _():
        stat_copy.wait_recv()

        @pl.when(x >= FAR)
        def _():
            attend_all()
            chain_all(True)

        @pl.when(x < FAR)
        def _():
            chain_all(False)
            attend_all()
            finish_all()

        for half in range(2):
            for slot in (8, 0, 1, 2, 3, 4, 5, 6, 7):
                core_copy(half, slot).wait_recv()

    @pl.when(core == 0)
    def _():
        attend_all()
        for half in range(2):
            for d in range(1, RING):
                first_in(half, d).wait_recv()
            for c in range(CUTS):
                for way in (1, -1):
                    ring_copy(half, way, 0, (c, CUTS - 1 - c)[way < 0]).start()
            core_copy(half, 8).start()
        for s in range(1, 5):
            for c in range(CUTS if s < 4 else CUTS // 2):
                for half in range(2):
                    for way in (1, -1):
                        cut = (c, CUTS - 1 - c)[way < 0]
                        ring_in(half, way, s, cut).wait_recv()
                        if s < 4 and cut in pieces(way, s + 1):
                            ring_copy(half, way, s, cut).start()
            for half in range(2):
                core_copy(half, 2 * s - 2).start()
                core_copy(half, 2 * s - 1).start()

        @pl.when(x > 0)
        def _():
            m_core.wait_recv()

        spread(4, m_eff[0:1, 0:PAIRS])

        def step(p, c):
            @pl.when(x > 0)
            def _():
                eff_copy(p, 0).wait_recv()
                eff_copy(p, 1).wait_recv()

            finish(p)
            return c

        lax.fori_loop(0, PAIRS, step, 0)

    def out_copy(i):
        cut = pl.ds(pl.multiple_of(i * 256, 256), 256)
        return pltpu.make_async_copy(o_ref.at[:, :, cut], o_hbm.at[:, :, cut], out_sem.at[i])

    def project(i, c):
        wt = wg[i].reshape(RING * 32, HEADS * DH)
        for b in range(2):
            o_ref[b, :, pl.ds(pl.multiple_of(i * 256, 256), 256)] = lax.dot_general(
                hid[b], wt, NT, preferred_element_type=F32
            ).astype(BF16)
        out_copy(i).start()
        return c

    lax.fori_loop(0, RING, project, 0)

    @pl.when(core == 0)
    def _():
        stat_copy.wait_send()
        for half in range(2):
            for d in range(1, RING):
                first(half, d).wait_send()
            for way in (1, -1):
                for s in range(4):
                    for c in pieces(way, s + 1):
                        ring_copy(half, way, s, c).wait_send()
            for slot in range(9):
                core_copy(half, slot).wait_send()

        def drain(p, c):
            loc_copy(p).wait_send()
            return c

        lax.fori_loop(0, PAIRS, drain, 0)

    @pl.when(core == 1)
    def _():
        @pl.when(x > 0)
        def _():
            m_core.wait_send()

        @pl.when(x < RING - 1)
        def _():
            m_right.wait_send()

        def drain(p, c):
            @pl.when(x > 0)
            def _():
                eff_copy(p, 0).wait_send()
                eff_copy(p, 1).wait_send()

            @pl.when(x < RING - 1)
            def _():
                chain_copy(p, 0).wait_send()
                chain_copy(p, 1).wait_send()

            return c

        lax.fori_loop(0, PAIRS, drain, 0)

    def written(i, c):
        out_copy(i).wait()
        return c

    lax.fori_loop(0, RING, written, 0)


def body(queries, keys, values, in_gate, forget_gate, out_gate, norm_gain, out_weight):
    seqs, heads, span, dh = queries.shape

    def by_pair(a):
        return a.reshape((PAIRS,) + a.shape[2:])

    hbm = pl.BlockSpec(memory_space=pltpu.HBM)
    dma = pltpu.SemaphoreType.DMA
    return pl.pallas_call(
        kernel,
        name="cell",
        out_shape=jax.ShapeDtypeStruct((seqs, span, 2048), BF16),
        in_specs=[hbm] * 8,
        out_specs=hbm,
        scratch_shapes=[
            pltpu.VMEM((PAIRS, T, DH), BF16),
            pltpu.VMEM((PAIRS, T, DH), BF16),
            pltpu.VMEM((PAIRS, T, DH), BF16),
            pltpu.VMEM((PAIRS, T), BF16),
            pltpu.VMEM((PAIRS, T), BF16),
            pltpu.VMEM((PAIRS, T, DH), BF16),
            pltpu.VMEM((HEADS, DH), F32),
            pltpu.VMEM((seqs, span, 2048), BF16),
            dma((8,)),
            dma((8,)),
            pltpu.VMEM((RING, RING, 32, heads * dh), BF16),
            pltpu.VMEM((PAIRS, SROWS, DH), BF16),
            pltpu.VMEM((PAIRS, SROWS, DH), BF16),
            pltpu.VMEM((PAIRS, SROWS, DH), BF16),
            pltpu.VMEM((PAIRS, SROWS, DH), F32),
            pltpu.VMEM((PAIRS, SROWS, DH), F32),
            pltpu.VMEM((PAIRS, T, DH), F32),
            pltpu.VMEM((PAIRS, T, DH), F32),
            pltpu.VMEM((PAIRS, T, DH), F32),
            pltpu.VMEM((2, T, heads * dh), BF16),
            pltpu.VMEM((PAIRS, T), F32),
            pltpu.VMEM((PAIRS, T, DH), F32),
            pltpu.VMEM((8, DH), F32),
            pltpu.VMEM((8, DH), F32),
            pltpu.VMEM((8, DH), F32),
            pltpu.VMEM((8, DH), F32),
            pltpu.VMEM((8, DH), F32),
            pltpu.VMEM((5, PAIRS, DH), F32),
            dma((2, 7)),
            dma((2, 7)),
            dma((4, 4 * CUTS)),
            dma((4, 4 * CUTS)),
            dma((2, 9)),
            dma((2, 9)),
            dma((PAIRS,)),
            dma((PAIRS,)),
            dma((PAIRS, 2)),
            dma((PAIRS, 2)),
            dma((PAIRS, 2)),
            dma((PAIRS, 2)),
            dma((3,)),
            dma((3,)),
        ],
        compiler_params=pltpu.CompilerParams(
            collective_id=0, has_side_effects=True, vmem_limit_bytes=60 * 2**20
        ),
    )(
        by_pair(queries), by_pair(keys), by_pair(values), by_pair(in_gate), by_pair(forget_gate),
        by_pair(out_gate), norm_gain, out_weight.T,
    )


def solution(mesh):
    finer = Mesh(mesh.devices.reshape(8, 2, 8, 8), ("x", "c", "z", "y"))
    sp, dp = ("x", "c"), ("z", "y")
    placed = (
        P(dp, None, sp, None),
        P(dp, None, sp, None),
        P(dp, None, sp, None),
        P(dp, None, sp),
        P(dp, None, sp),
        P(dp, None, sp, None),
        P(),
        P(None, dp),
    )
    return jax.shard_map(
        body, mesh=finer, in_specs=placed, out_specs=P(dp, sp, None), check_vma=False
    )
```

profile of v0, /device:TPU:14, one launch (start us, length us, event | category | flops | bytes accessed | tf_op | source)
XLA Modules:
  0.0 61.4 jit_solution(14731292368990029116)
XLA Ops:
  0.0 59.0 %cell.1 = bf16[2,144,2048]{2,1,0:T(8,128)(2,1)} custom-call(bf16[16,144,128]{2,1,0:T(8,128)(2,1)} %bitcast.7, bf16[16,144,128]{2,1,0:T(8,128)(2,1)} %bitcast.8, bf16[16,144,128]{2,1,0:T(8,128)(2,1)} %bitcast.9, bf16[16,144]{1,0:T(8,128)(2,1)} %bitcast.12, bf16[16,144]{1,0:T(8,128)(2,1)} %bitcast.13, bf16[16,144,128]{2,1,0:T(8,128)(2,1)} %bitcast.10, ...), custom_call_target="tpu_custom_call" | custom-call | tf_op jit(solution)/shard_map/cell/pallas_call | solution.py:491
  59.0 2.4 %copy.10 = bf16[2,144,2048]{2,1,0:T(8,128)(2,1)} copy(bf16[2,144,2048]{2,1,0:T(8,128)(2,1)} %cell.1) | data formatting | bytes 2359296
where the time goes:
time: 61.6 us; the launch traced here: 61.4 us
  Pallas kernels  59 us (96%)
  local copies, waits for them, and re-layouts  2.41 us (4%)
    pallas_call x1, Pallas kernels, body(): pl.pallas_call(kernel, name='cell', out_shape=jax.ShapeDtypeStruct((seqs,...  59 us
    unnamed x1, local copies, waits for them, and re-layouts  2.41 us

commit v1 on v0

v1 whole, which is shorter than its diff:
```python
import functools

import jax
import jax.numpy as jnp
from jax import lax
from jax.experimental import pallas as pl
from jax.experimental.pallas import tpu as pltpu
from jax.sharding import Mesh
from jax.sharding import PartitionSpec as P

SC = jax.named_scope
MESH = pl.DeviceIdType.MESH
F32 = jnp.float32
BF16 = jnp.bfloat16
HI = lax.Precision.HIGHEST
NT = (((1,), (1,)), ((), ()))
TN = (((0,), (0,)), ((), ()))
EPS = 1e-05
HEADS = 8
PAIRS = 16
T = 144
DH = 128
SROWS = 144
RING = 8
PARTS = ((0, 80), (80, 64))
CUTS = 4
FAR = 2


def kernel(
    q_hbm, k_hbm, v_hbm, ig_hbm, fg_hbm, og_hbm, gain_hbm, w_hbm, o_ref,
    q_ref, k_ref, v_ref, ig_ref, fg_ref, og_ref, gain_ref, in_sem,
    wg, state_in, state_out, state_eff, local, peer_local, num_loc, den_loc, top, gates, hid,
    arow, wcol, stat, peer_stat, m_in, m_out, m_eff, coef,
    one_send, one_recv, ring_send, ring_recv, core_w_send, core_w_recv,
    loc_send, loc_recv, ch_send, ch_recv, eff_send, eff_recv, small_send, small_recv,
):
    x = lax.axis_index("x")
    core = lax.axis_index("c")
    z = lax.axis_index("z")
    y = lax.axis_index("y")
    other = {"c": 1 - core}
    barrier = pltpu.get_barrier_semaphore()

    def at(axis, d):
        return {axis: lax.rem(lax.axis_index(axis) + (d + RING), RING)}

    def copy(src, dst, ss, rs, dev):
        return pltpu.make_async_remote_copy(
            src_ref=src, dst_ref=dst, send_sem=ss, recv_sem=rs, device_id=dev, device_id_type=MESH
        )

    def drain(ref, sem):
        pltpu.make_async_copy(ref, ref, sem).wait()

    def greet(dev):
        pl.semaphore_signal(barrier, inc=1, device_id=dev, device_id_type=MESH)

    greet(other)

    @pl.when(core == 0)
    def _():
        for axis in ("y", "z"):
            for d in range(1, RING):
                greet(at(axis, d))

    @pl.when(core == 1)
    def _():
        greet(at("x", 1))
        greet(at("x", -1))

    loads = [
        pltpu.make_async_copy(src, dst, in_sem.at[i])
        for i, (src, dst) in enumerate(
            (
                (fg_hbm, fg_ref),
                (ig_hbm, ig_ref),
                (k_hbm, k_ref),
                (v_hbm, v_ref),
                (q_hbm, q_ref),
                (og_hbm, og_ref),
                (gain_hbm, gain_ref),
            )
        )
    ]
    w_load = pltpu.make_async_copy(w_hbm, wg.at[z, y], in_sem.at[7])
    for load in loads[:2]:
        load.start()

    @pl.when(core == 0)
    def _():
        w_load.start()

    for load in loads[2:]:
        load.start()

    row_i = lax.broadcasted_iota(jnp.int32, (T, T), 0)
    col_i = lax.broadcasted_iota(jnp.int32, (T, T), 1)
    lower = (col_i <= row_i).astype(BF16)
    eye = (col_i == row_i).astype(BF16)
    loads[0].wait()
    loads[1].wait()
    logf = -jnp.log1p(jnp.exp(-fg_ref[...].astype(F32)))
    rest = logf
    sum_t = jnp.zeros((T, PAIRS), F32)
    sum_r = jnp.zeros((PAIRS, T), F32)
    for _ in range(3):
        term = rest.astype(BF16)
        rest = rest - term.astype(F32)
        sum_t = sum_t + lax.dot_general(lower, term, NT, preferred_element_type=F32)
        sum_r = sum_r + lax.dot_general(term, lower, NT, preferred_element_type=F32)
    inp = ig_ref[...].astype(F32)
    inp_t = lax.dot_general(eye, ig_ref[...], NT, preferred_element_type=F32)
    arow[...] = inp - sum_r
    a_t = inp_t - sum_t
    top_row = jnp.max(a_t, axis=0, keepdims=True)
    w_t = jnp.exp(a_t - top_row) * (DH**-0.5)
    for p in range(PAIRS):
        wcol[p] = jnp.broadcast_to(w_t[:, p : p + 1], (T, DH))
    stat[0:1, 0:PAIRS] = sum_t[T - 1 : T, :]
    stat[1:2, 0:PAIRS] = top_row

    def first(half, d):
        axis = ("y", "z")[half]
        ref = wg.at[z, y, pl.ds(16 * half, 16)]
        return copy(ref, ref, one_send, one_recv.at[half], at(axis, d))

    def block(half, n):
        return wg.at[n, :, pl.ds(0, 16)] if half == 0 else wg.at[:, n, pl.ds(16, 16)]

    def second_axis(half):
        return ("z", "y")[half]

    def shifted(half, d):
        return lax.rem(lax.axis_index(second_axis(half)) + (d + RING), RING)

    def piece(half, way, s, c):
        cut = pl.ds(c * (RING // CUTS), RING // CUTS)
        n = shifted(half, -way * s)
        return wg.at[n, cut, pl.ds(0, 16)] if half == 0 else wg.at[cut, n, pl.ds(16, 16)]

    def pieces(way, s):
        return range(CUTS) if s < 4 else (range(CUTS // 2), range(CUTS // 2, CUTS))[way < 0]

    def ring_copy(half, way, s, c):
        ref = piece(half, way, s, c)
        f, i = 2 * half + (way < 0), CUTS * s + c
        return copy(ref, ref, ring_send, ring_recv.at[f, i], at(second_axis(half), way))

    def ring_in(half, way, s, c):
        ref = piece(half, way, s, c)
        f, i = 2 * half + (way < 0), CUTS * (s - 1) + c
        return copy(ref, ref, ring_send, ring_recv.at[f, i], at(second_axis(half), way))

    def core_copy(ref):
        return copy(ref, ref, core_w_send, core_w_recv, other)

    stat_copy = copy(stat, peer_stat, small_send.at[0], small_recv.at[0], other)
    m_right = copy(m_out, m_in, small_send.at[1], small_recv.at[1], at("x", 1))
    m_core = copy(m_in, m_eff, small_send.at[2], small_recv.at[2], other)

    def loc_copy(g):
        group = pl.ds(4 * g, 4)
        return copy(local.at[group], peer_local.at[group], loc_send, loc_recv.at[g], other)

    def chain_copy(p, h):
        rows = pl.ds(*PARTS[h])
        return copy(
            state_out.at[p, rows], state_in.at[p, rows], ch_send, ch_recv.at[p, h], at("x", 1)
        )

    def eff_copy(p, h):
        rows = pl.ds(*PARTS[h])
        return copy(state_in.at[p, rows], state_eff.at[p, rows], eff_send, eff_recv.at[lax.div(p, 2)], other)

    @pl.when(x == 0)
    def _():
        zero = jnp.zeros((8, DH), F32)
        m_in[...] = zero

        @pl.when(core == 0)
        def _():
            m_eff[...] = zero

        def clear(p, c):
            state_in[p] = jnp.zeros((SROWS, DH), BF16)

            @pl.when(core == 0)
            def _():
                state_eff[p] = jnp.zeros((SROWS, DH), BF16)

            return c

        lax.fori_loop(0, PAIRS, clear, 0)

    tail_i = lax.broadcasted_iota(jnp.int32, (16, DH), 0)

    def local_state(g, c):
        found = []
        for j in range(4):
            p = 4 * g + j
            kw = k_ref[p].astype(F32) * wcol[p]
            n = jnp.sum(kw, axis=0, keepdims=True)
            memory = lax.dot_general(v_ref[p], kw.astype(BF16), TN, preferred_element_type=F32)
            found.append((p, memory, jnp.where(tail_i == 0, jnp.broadcast_to(n, (16, DH)), 0.0)))
        for p, memory, tail in found:
            local[p, 0:DH] = memory
            local[p, DH:SROWS] = tail
        return c

    with SC("kv_in"):
        loads[2].wait()
        loads[3].wait()
    with SC("local"):
        lax.fori_loop(0, PAIRS // 4, local_state, 0)

    @pl.when(core == 1)
    def _():
        with SC("barrier"):
            pl.semaphore_wait(barrier, 3)

    @pl.when(core == 0)
    def _():
        with SC("barrier"):
            pl.semaphore_wait(barrier, 15)
        stat_copy.start()

        for g in range(4):
            loc_copy(g).start()
        w_load.wait()
        for d in (4, 3, 5, 2, 6, 1, 7):
            first(0, d).start()
            first(1, d).start()

    for load in loads[4:]:
        load.wait()

    def attend(g, c):
        found = []
        for j in range(2):
            p = 2 * g + j
            a = arow[pl.ds(p, 1), :]
            masked = jnp.where(col_i <= row_i, jnp.broadcast_to(a, (T, T)), -1e30)
            t = jnp.max(masked, axis=1, keepdims=True)
            wt = jnp.exp(masked - t) * (DH**-0.5)
            s = lax.dot_general(q_ref[p], k_ref[p], NT, preferred_element_type=F32) * wt
            high = s.astype(BF16)
            low = (s - high.astype(F32)).astype(BF16)
            num = jnp.dot(high, v_ref[p], preferred_element_type=F32) + jnp.dot(
                low, v_ref[p], preferred_element_type=F32
            )
            gate = 0.5 * jnp.tanh(0.5 * og_ref[p].astype(F32)) + 0.5
            gain = gain_ref[pl.ds(lax.rem(2 * g, HEADS) + j, 1), :]
            found.append((p, t, jnp.sum(s, axis=1, keepdims=True), num, gate * gain))
        for p, t, den, num, gate in found:
            gates[p] = gate
            top[p] = jnp.broadcast_to(t, (T, DH))
            den_loc[p] = jnp.broadcast_to(den, (T, DH))
            num_loc[p] = num
        return c

    def attend_all():
        with SC("attend"):
            lax.fori_loop(0, PAIRS // 2, attend, 0)

    def finish(g):
        h = lax.rem(2 * g, HEADS)
        rows = pl.ds(pl.multiple_of(lax.div(2 * g, HEADS) * T, T), T)
        found = []
        for j in range(2):
            p = 2 * g + j
            t = top[p]
            m = m_eff_b(p)
            mu = jnp.maximum(t, m)
            g1 = jnp.exp(m - mu)
            g2 = jnp.exp(t - mu)
            inter = lax.dot_general(q_ref[p], state_eff[p], NT, preferred_element_type=F32)
            num = g1 * inter[:, 0:DH] + g2 * num_loc[p]
            den = g1 * jnp.broadcast_to(inter[:, DH : DH + 1], (T, DH)) + g2 * den_loc[p]
            cell = (num / jnp.maximum(jnp.abs(den), 1.0)).astype(BF16).astype(F32)
            mean = jnp.mean(cell, axis=1, keepdims=True)
            cen = cell - mean
            var = jnp.mean(cen * cen, axis=1, keepdims=True)
            found.append((cen * lax.rsqrt(var + EPS) * gates[p]).astype(BF16))
        hid[rows, pl.ds(pl.multiple_of(h * DH, 2 * DH), 2 * DH)] = jnp.concatenate(found, axis=1)

    def m_eff_b(p):
        return coef[4, pl.ds(p, 1), :]

    eye_p = lax.broadcasted_iota(jnp.int32, (PAIRS, PAIRS), 0) == lax.broadcasted_iota(
        jnp.int32, (PAIRS, PAIRS), 1
    )

    def spread(i, row):
        column = jnp.sum(jnp.where(eye_p, jnp.broadcast_to(row, (PAIRS, PAIRS)), 0.0), axis=1, keepdims=True)
        coef[i] = jnp.broadcast_to(column, (PAIRS, DH))

    def chain(p):
        c_old, c_peer = coef[0, pl.ds(p, 1), :], coef[1, pl.ds(p, 1), :]
        c_mid, c_own = coef[2, pl.ds(p, 1), :], coef[3, pl.ds(p, 1), :]
        for h, (row, n) in enumerate(PARTS):
            rows = pl.ds(row, n)
            mid = c_peer * peer_local[p, rows]
            out = c_mid * mid + c_own * local[p, rows]

            @pl.when(x > 0)
            def _():
                with SC("ch_wait"):
                    chain_copy(p, h).wait_recv()
                eff_copy(p, h).start()

            old = c_old * state_in[p, rows].astype(F32)
            state_out[p, rows] = (c_mid * old + out).astype(BF16)

            @pl.when(x < RING - 1)
            def _():
                chain_copy(p, h).start()

            state_eff[p, rows] = (old + mid).astype(BF16)

    def chain_all(with_finish):
        @pl.when(x > 0)
        def _():
            with SC("m_right"):
                m_right.wait_recv()

        e0, t0 = peer_stat[0:1, 0:PAIRS], peer_stat[1:2, 0:PAIRS]
        e1, t1 = stat[0:1, 0:PAIRS], stat[1:2, 0:PAIRS]
        m0 = m_in[0:1, 0:PAIRS]
        mu0 = jnp.maximum(m0, t0)
        m1 = e0 + mu0
        mu1 = jnp.maximum(m1, t1)
        m_out[0:1, 0:PAIRS] = e1 + mu1

        @pl.when(x < RING - 1)
        def _():
            m_right.start()

        @pl.when(x > 0)
        def _():
            m_core.start()

        spread(0, jnp.exp(m0 - mu0))
        spread(1, jnp.exp(t0 - mu0))
        spread(2, jnp.exp(m1 - mu1))
        spread(3, jnp.exp(t1 - mu1))
        spread(4, m1)

        def step(g, c):
            loc_copy(g).wait_recv()
            for j in range(2):
                chain(4 * g + 2 * j)
                chain(4 * g + 2 * j + 1)
                if with_finish:
                    finish(2 * g + j)
            return c

        lax.fori_loop(0, PAIRS // 4, step, 0)

    def finish_all():
        def step(g, c):
            finish(g)
            return c

        with SC("finish"):
            lax.fori_loop(0, PAIRS // 2, step, 0)

    @pl.when(core == 1)
    def _():
        with SC("stat"):
            stat_copy.wait_recv()

        @pl.when(x >= FAR)
        def _():
            attend_all()
            chain_all(True)

        @pl.when(x < FAR)
        def _():
            chain_all(False)
            attend_all()
            finish_all()

        with SC("w_wait"):
            drain(wg, core_w_recv)

    @pl.when(core == 0)
    def _():
        attend_all()
        for half in range(2):
            with SC("first"):
                drain(wg.at[pl.ds(0, RING - 1), 0, pl.ds(0, 16)], one_recv.at[half])
            for c in range(CUTS):
                for way in (1, -1):
                    ring_copy(half, way, 0, (c, CUTS - 1 - c)[way < 0]).start()
            core_copy(block(half, shifted(half, 0))).start()
        for s in range(1, 5):
            with SC("ring"):
                for c in range(CUTS if s < 4 else CUTS // 2):
                    for half in range(2):
                        for way in (1, -1):
                            cut = (c, CUTS - 1 - c)[way < 0]
                            ring_in(half, way, s, cut).wait_recv()
                            if s < 4 and cut in pieces(way, s + 1):
                                ring_copy(half, way, s, cut).start()
                            core_copy(piece(half, way, s, cut)).start()

        @pl.when(x > 0)
        def _():
            m_core.wait_recv()

        spread(4, m_eff[0:1, 0:PAIRS])

        def step(g, c):
            @pl.when(x > 0)
            def _():
                with SC("eff_wait"):
                    drain(state_eff.at[pl.ds(2 * g, 2)], eff_recv.at[g])

            finish(g)
            return c

        lax.fori_loop(0, PAIRS // 2, step, 0)

    def project(i, c):
        for j in range(2):
            n = 2 * i + j
            wt = wg[n].reshape(RING * 32, HEADS * DH)
            cut = pl.ds(pl.multiple_of(n * 256, 256), 256)
            res = lax.dot_general(hid[...], wt, NT, preferred_element_type=F32).astype(BF16)
            o_ref[0, :, cut] = res[0:T]
            o_ref[1, :, cut] = res[T:]
        return c

    with SC("project"):
        lax.fori_loop(0, RING // 2, project, 0)

    @pl.when(core == 0)
    def _():
        stat_copy.wait_send()
        drain(local, loc_send)
        drain(wg.at[pl.ds(0, RING - 1), pl.ds(0, 2), pl.ds(0, 16)], one_send)
        drain(wg.at[pl.ds(0, RING - 1)], ring_send)
        drain(wg, core_w_send)

    @pl.when(core == 1)
    def _():
        @pl.when(x > 0)
        def _():
            m_core.wait_send()
            drain(state_in, eff_send)

        @pl.when(x < RING - 1)
        def _():
            m_right.wait_send()
            drain(state_out, ch_send)


def body(queries, keys, values, in_gate, forget_gate, out_gate, norm_gain, out_weight):
    seqs, heads, span, dh = queries.shape

    def by_pair(a):
        return a.reshape((PAIRS,) + a.shape[2:])

    hbm = pl.BlockSpec(memory_space=pltpu.HBM)
    dma = pltpu.SemaphoreType.DMA
    return pl.pallas_call(
        kernel,
        name="cell",
        out_shape=pltpu.VMEM((seqs, span, 2048), BF16),
        in_specs=[hbm] * 8,
        out_specs=pl.BlockSpec(memory_space=pltpu.VMEM),
        scratch_shapes=[
            pltpu.VMEM((PAIRS, T, DH), BF16),
            pltpu.VMEM((PAIRS, T, DH), BF16),
            pltpu.VMEM((PAIRS, T, DH), BF16),
            pltpu.VMEM((PAIRS, T), BF16),
            pltpu.VMEM((PAIRS, T), BF16),
            pltpu.VMEM((PAIRS, T, DH), BF16),
            pltpu.VMEM((HEADS, DH), F32),
            dma((8,)),
            pltpu.VMEM((RING, RING, 32, heads * dh), BF16),
            pltpu.VMEM((PAIRS, SROWS, DH), BF16),
            pltpu.VMEM((PAIRS, SROWS, DH), BF16),
            pltpu.VMEM((PAIRS, SROWS, DH), BF16),
            pltpu.VMEM((PAIRS, SROWS, DH), F32),
            pltpu.VMEM((PAIRS, SROWS, DH), F32),
            pltpu.VMEM((PAIRS, T, DH), F32),
            pltpu.VMEM((PAIRS, T, DH), F32),
            pltpu.VMEM((PAIRS, T, DH), F32),
            pltpu.VMEM((PAIRS, T, DH), F32),
            pltpu.VMEM((2 * T, heads * dh), BF16),
            pltpu.VMEM((PAIRS, T), F32),
            pltpu.VMEM((PAIRS, T, DH), F32),
            pltpu.VMEM((8, DH), F32),
            pltpu.VMEM((8, DH), F32),
            pltpu.VMEM((8, DH), F32),
            pltpu.VMEM((8, DH), F32),
            pltpu.VMEM((8, DH), F32),
            pltpu.VMEM((5, PAIRS, DH), F32),
            dma,
            dma((2,)),
            dma,
            dma((4, 4 * CUTS)),
            dma,
            dma,
            dma,
            dma((4,)),
            dma,
            dma((PAIRS, 2)),
            dma,
            dma((PAIRS // 2,)),
            dma((3,)),
            dma((3,)),
        ],
        compiler_params=pltpu.CompilerParams(
            collective_id=0, has_side_effects=True, vmem_limit_bytes=60 * 2**20
        ),
    )(
        by_pair(queries), by_pair(keys), by_pair(values), by_pair(in_gate), by_pair(forget_gate),
        by_pair(out_gate), norm_gain, out_weight.T,
    )


def solution(mesh):
    finer = Mesh(mesh.devices.reshape(8, 2, 8, 8), ("x", "c", "z", "y"))
    sp, dp = ("x", "c"), ("z", "y")
    placed = (
        P(dp, None, sp, None),
        P(dp, None, sp, None),
        P(dp, None, sp, None),
        P(dp, None, sp),
        P(dp, None, sp),
        P(dp, None, sp, None),
        P(),
        P(None, dp),
    )
    return jax.shard_map(
        body, mesh=finer, in_specs=placed, out_specs=P(dp, sp, None), check_vma=False
    )
```

time: 61.6 us -> 50.6 us (0.82)
  Pallas kernels: 59 us -> 49.4 us
  local copies, waits for them, and re-layouts: 2.41 us -> 1.02 us
    pallas_call x1, Pallas kernels: 59 us -> 49.4 us  [body(): pl.pallas_call(kernel, name='cell', out_shape=pltpu.VMEM((seqs, span, 204...]
    unnamed x1, local copies, waits for them, and re-layouts: 2.41 us -> 1.02 us
where the time goes in v1:
time: 50.6 us; the launch traced here: 50.4 us
  Pallas kernels  49.4 us (98%)
  local copies, waits for them, and re-layouts  1.02 us (2%)
    pallas_call x1, Pallas kernels, body(): pl.pallas_call(kernel, name='cell', out_shape=pltpu.VMEM((seqs, span, 204...  49.4 us
    unnamed x1, local copies, waits for them, and re-layouts  1.02 us

profile of v1, /device:TPU:14, one launch (start us, length us, event | category | flops | bytes accessed | tf_op | source)
XLA Modules:
  0.0 50.4 jit_solution(2079979688404193067)
XLA Ops:
  0.0 49.4 %cell.1 = bf16[2,144,2048]{2,1,0:T(8,128)(2,1)S(1)} custom-call(bf16[16,144,128]{2,1,0:T(8,128)(2,1)} %bitcast.7, bf16[16,144,128]{2,1,0:T(8,128)(2,1)} %bitcast.8, bf16[16,144,128]{2,1,0:T(8,128)(2,1)} %bitcast.9, bf16[16,144]{1,0:T(8,128)(2,1)} %bitcast.12, bf16[16,144]{1,0:T(8,128)(2,1)} %bitcast.13, bf16[16,144,128]{2,1,0:T(8,128)(2,1)} %bitcast.10, ...), custom_call_target="tpu_custom_call" | custom-call | tf_op jit(solution)/shard_map/cell/pallas_call | solution.py:467
  49.4 1.0 %copy.10 = bf16[2,144,2048]{2,1,0:T(8,128)(2,1)} copy(bf16[2,144,2048]{2,1,0:T(8,128)(2,1)S(1)} %cell.1) | data formatting | bytes 2359296

commit v2 on v1

--- a/solution.py
+++ b/solution.py
@@ -22,7 +22,7 @@
 DH = 128
 SROWS = 144
 RING = 8
-PARTS = ((0, 80), (80, 64))
+PARTS = ((0, 64), (64, 64))
 CUTS = 4
 FAR = 2
 
@@ -31,7 +31,7 @@
     q_hbm, k_hbm, v_hbm, ig_hbm, fg_hbm, og_hbm, gain_hbm, w_hbm, o_ref,
     q_ref, k_ref, v_ref, ig_ref, fg_ref, og_ref, gain_ref, in_sem,
     wg, state_in, state_out, state_eff, local, peer_local, num_loc, den_loc, top, gates, hid,
-    arow, wcol, stat, peer_stat, m_in, m_out, m_eff, coef,
+    arow, wcol, stat, peer_stat, m_in, m_out, m_eff, n_in, n_out, n_eff, coef,
     one_send, one_recv, ring_send, ring_recv, core_w_send, core_w_recv,
     loc_send, loc_recv, ch_send, ch_recv, eff_send, eff_recv, small_send, small_recv,
 ):
@@ -144,12 +144,12 @@
 
     def ring_copy(half, way, s, c):
         ref = piece(half, way, s, c)
-        f, i = 2 * half + (way < 0), CUTS * s + c
+        f, i = 2 * half + (way < 0), CUTS * s + (c if s < 3 else c % 2)
         return copy(ref, ref, ring_send, ring_recv.at[f, i], at(second_axis(half), way))
 
     def ring_in(half, way, s, c):
         ref = piece(half, way, s, c)
-        f, i = 2 * half + (way < 0), CUTS * (s - 1) + c
+        f, i = 2 * half + (way < 0), CUTS * (s - 1) + (c if s < 4 else c % 2)
         return copy(ref, ref, ring_send, ring_recv.at[f, i], at(second_axis(half), way))
 
     def core_copy(ref):
@@ -158,6 +158,8 @@
     stat_copy = copy(stat, peer_stat, small_send.at[0], small_recv.at[0], other)
     m_right = copy(m_out, m_in, small_send.at[1], small_recv.at[1], at("x", 1))
     m_core = copy(m_in, m_eff, small_send.at[2], small_recv.at[2], other)
+    n_right = copy(n_out, n_in, small_send.at[3], small_recv.at[3], at("x", 1))
+    n_core = copy(n_in, n_eff, small_send.at[4], small_recv.at[4], other)
 
     def loc_copy(g):
         group = pl.ds(4 * g, 4)
@@ -177,17 +179,19 @@
     def _():
         zero = jnp.zeros((8, DH), F32)
         m_in[...] = zero
+        n_in[...] = jnp.zeros((PAIRS, DH), F32)
 
         @pl.when(core == 0)
         def _():
             m_eff[...] = zero
+            n_eff[...] = jnp.zeros((PAIRS, DH), F32)
 
         def clear(p, c):
-            state_in[p] = jnp.zeros((SROWS, DH), BF16)
+            state_in[p] = jnp.zeros((DH, DH), BF16)
 
             @pl.when(core == 0)
             def _():
-                state_eff[p] = jnp.zeros((SROWS, DH), BF16)
+                state_eff[p, 0:DH] = jnp.zeros((DH, DH), BF16)
 
             return c
 
@@ -202,10 +206,10 @@
             kw = k_ref[p].astype(F32) * wcol[p]
             n = jnp.sum(kw, axis=0, keepdims=True)
             memory = lax.dot_general(v_ref[p], kw.astype(BF16), TN, preferred_element_type=F32)
-            found.append((p, memory, jnp.where(tail_i == 0, jnp.broadcast_to(n, (16, DH)), 0.0)))
-        for p, memory, tail in found:
-            local[p, 0:DH] = memory
-            local[p, DH:SROWS] = tail
+            found.append((p, memory, n))
+        for p, memory, n in found:
+            local[p] = memory
+            stat[pl.ds(8 + p, 1), :] = n
         return c
 
     with SC("kv_in"):
@@ -263,12 +267,12 @@
         with SC("attend"):
             lax.fori_loop(0, PAIRS // 2, attend, 0)
 
-    def finish(g):
-        h = lax.rem(2 * g, HEADS)
-        rows = pl.ds(pl.multiple_of(lax.div(2 * g, HEADS) * T, T), T)
+    def finish(begin, count):
+        h = lax.rem(begin, HEADS)
+        rows = pl.ds(pl.multiple_of(lax.div(begin, HEADS) * T, T), T)
         found = []
-        for j in range(2):
-            p = 2 * g + j
+        for j in range(count):
+            p = begin + j
             t = top[p]
             m = m_eff_b(p)
             mu = jnp.maximum(t, m)
@@ -282,7 +286,8 @@
             cen = cell - mean
             var = jnp.mean(cen * cen, axis=1, keepdims=True)
             found.append((cen * lax.rsqrt(var + EPS) * gates[p]).astype(BF16))
-        hid[rows, pl.ds(pl.multiple_of(h * DH, 2 * DH), 2 * DH)] = jnp.concatenate(found, axis=1)
+        cut = pl.ds(pl.multiple_of(h * DH, count * DH), count * DH)
+        hid[rows, cut] = jnp.concatenate(found, axis=1)
 
     def m_eff_b(p):
         return coef[4, pl.ds(p, 1), :]
@@ -318,6 +323,14 @@
 
             state_eff[p, rows] = (old + mid).astype(BF16)
 
+    def fill_tails():
+        def step(p, c):
+            n = jnp.broadcast_to(n_eff[pl.ds(p, 1), :], (16, DH))
+            state_eff[p, DH:SROWS] = jnp.where(tail_i == 0, n, 0.0).astype(BF16)
+            return c
+
+        lax.fori_loop(0, PAIRS, step, 0)
+
     def chain_all(with_finish):
         @pl.when(x > 0)
         def _():
@@ -346,24 +359,39 @@
         spread(3, jnp.exp(t1 - mu1))
         spread(4, m1)
 
+        @pl.when(x > 0)
+        def _():
+            n_right.wait_recv()
+            n_core.start()
+
+        n_mid = coef[0] * n_in[...] + coef[1] * peer_stat[8:24, :]
+        n_out[...] = coef[2] * n_mid + coef[3] * stat[8:24, :]
+        n_eff[...] = n_mid
+
+        @pl.when(x < RING - 1)
+        def _():
+            n_right.start()
+
+        fill_tails()
+
         def step(g, c):
             loc_copy(g).wait_recv()
             for j in range(2):
                 chain(4 * g + 2 * j)
                 chain(4 * g + 2 * j + 1)
                 if with_finish:
-                    finish(2 * g + j)
+                    finish(4 * g + 2 * j, 2)
             return c
 
         lax.fori_loop(0, PAIRS // 4, step, 0)
 
     def finish_all():
         def step(g, c):
-            finish(g)
+            finish(4 * g, 4)
             return c
 
         with SC("finish"):
-            lax.fori_loop(0, PAIRS // 2, step, 0)
+            lax.fori_loop(0, PAIRS // 4, step, 0)
 
     @pl.when(core == 1)
     def _():
@@ -411,16 +439,28 @@
 
         spread(4, m_eff[0:1, 0:PAIRS])
 
-        def step(g, c):
+        @pl.when(x > 0)
+        def _():
+            n_core.wait_recv()
+
+        fill_tails()
+
+        def arrived(g):
             @pl.when(x > 0)
             def _():
                 with SC("eff_wait"):
-                    drain(state_eff.at[pl.ds(2 * g, 2)], eff_recv.at[g])
-
-            finish(g)
+                    drain(state_in.at[pl.ds(2 * g, 2)], eff_recv.at[g])
+
+        def step(g, c):
+            arrived(2 * g)
+            arrived(2 * g + 1)
+            finish(4 * g, 4)
             return c
 
-        lax.fori_loop(0, PAIRS // 2, step, 0)
+        lax.fori_loop(0, PAIRS // 4 - 1, step, 0)
+        for g in (PAIRS // 2 - 2, PAIRS // 2 - 1):
+            arrived(g)
+            finish(2 * g, 2)
 
     def project(i, c):
         for j in range(2):
@@ -448,11 +488,13 @@
         @pl.when(x > 0)
         def _():
             m_core.wait_send()
+            n_core.wait_send()
             drain(state_in, eff_send)
 
         @pl.when(x < RING - 1)
         def _():
             m_right.wait_send()
+            n_right.wait_send()
             drain(state_out, ch_send)
 
 
@@ -480,11 +522,11 @@
             pltpu.VMEM((HEADS, DH), F32),
             dma((8,)),
             pltpu.VMEM((RING, RING, 32, heads * dh), BF16),
+            pltpu.VMEM((PAIRS, DH, DH), BF16),
+            pltpu.VMEM((PAIRS, DH, DH), BF16),
             pltpu.VMEM((PAIRS, SROWS, DH), BF16),
-            pltpu.VMEM((PAIRS, SROWS, DH), BF16),
-            pltpu.VMEM((PAIRS, SROWS, DH), BF16),
-            pltpu.VMEM((PAIRS, SROWS, DH), F32),
-            pltpu.VMEM((PAIRS, SROWS, DH), F32),
+            pltpu.VMEM((PAIRS, DH, DH), F32),
+            pltpu.VMEM((PAIRS, DH, DH), F32),
             pltpu.VMEM((PAIRS, T, DH), F32),
             pltpu.VMEM((PAIRS, T, DH), F32),
             pltpu.VMEM((PAIRS, T, DH), F32),
@@ -492,16 +534,19 @@
             pltpu.VMEM((2 * T, heads * dh), BF16),
             pltpu.VMEM((PAIRS, T), F32),
             pltpu.VMEM((PAIRS, T, DH), F32),
+            pltpu.VMEM((24, DH), F32),
+            pltpu.VMEM((24, DH), F32),
             pltpu.VMEM((8, DH), F32),
             pltpu.VMEM((8, DH), F32),
             pltpu.VMEM((8, DH), F32),
-            pltpu.VMEM((8, DH), F32),
-            pltpu.VMEM((8, DH), F32),
+            pltpu.VMEM((PAIRS, DH), F32),
+            pltpu.VMEM((PAIRS, DH), F32),
+            pltpu.VMEM((PAIRS, DH), F32),
             pltpu.VMEM((5, PAIRS, DH), F32),
             dma,
             dma((2,)),
             dma,
-            dma((4, 4 * CUTS)),
+            dma((4, 3 * CUTS + CUTS // 2)),
             dma,
             dma,
             dma,
@@ -510,8 +555,8 @@
             dma((PAIRS, 2)),
             dma,
             dma((PAIRS // 2,)),
-            dma((3,)),
-            dma((3,)),
+            dma((5,)),
+            dma((5,)),
         ],
         compiler_params=pltpu.CompilerParams(
             collective_id=0, has_side_effects=True, vmem_limit_bytes=60 * 2**20

time: 50.6 us -> 49.5 us (0.978)
  Pallas kernels: 49.4 us -> 48.3 us
    pallas_call x1, Pallas kernels: 49.4 us -> 48.3 us  [body(): pl.pallas_call(kernel, name='cell', out_shape=pltpu.VMEM((seqs, span, 204...]
where the time goes in v2:
time: 49.5 us; the launch traced here: 49.3 us
  Pallas kernels  48.3 us (98%)
  local copies, waits for them, and re-layouts  1.02 us (2%)
    pallas_call x1, Pallas kernels, body(): pl.pallas_call(kernel, name='cell', out_shape=pltpu.VMEM((seqs, span, 204...  48.3 us
    unnamed x1, local copies, waits for them, and re-layouts  1.02 us

profile of v2, /device:TPU:14, one launch (start us, length us, event | category | flops | bytes accessed | tf_op | source)
XLA Modules:
  0.0 49.3 jit_solution(14971797213654694110)
XLA Ops:
  0.0 48.3 %cell.1 = bf16[2,144,2048]{2,1,0:T(8,128)(2,1)S(1)} custom-call(bf16[16,144,128]{2,1,0:T(8,128)(2,1)} %bitcast.7, bf16[16,144,128]{2,1,0:T(8,128)(2,1)} %bitcast.8, bf16[16,144,128]{2,1,0:T(8,128)(2,1)} %bitcast.9, bf16[16,144]{1,0:T(8,128)(2,1)} %bitcast.12, bf16[16,144]{1,0:T(8,128)(2,1)} %bitcast.13, bf16[16,144,128]{2,1,0:T(8,128)(2,1)} %bitcast.10, ...), custom_call_target="tpu_custom_call" | custom-call | tf_op jit(solution)/shard_map/cell/pallas_call | solution.py:509
  48.3 1.0 %copy.10 = bf16[2,144,2048]{2,1,0:T(8,128)(2,1)} copy(bf16[2,144,2048]{2,1,0:T(8,128)(2,1)S(1)} %cell.1) | data formatting | bytes 2359296

commit v3 on v2

--- a/solution.py
+++ b/solution.py
@@ -463,8 +463,8 @@
             finish(2 * g, 2)
 
     def project(i, c):
-        for j in range(2):
-            n = 2 * i + j
+        for j in range(4):
+            n = 4 * i + j
             wt = wg[n].reshape(RING * 32, HEADS * DH)
             cut = pl.ds(pl.multiple_of(n * 256, 256), 256)
             res = lax.dot_general(hid[...], wt, NT, preferred_element_type=F32).astype(BF16)
@@ -473,7 +473,7 @@
         return c
 
     with SC("project"):
-        lax.fori_loop(0, RING // 2, project, 0)
+        lax.fori_loop(0, RING // 4, project, 0)
 
     @pl.when(core == 0)
     def _():

time: 49.5 us -> 49 us (0.990)
  Pallas kernels: 48.3 us -> 47.8 us
where the time goes in v3:
time: 49 us; the launch traced here: 48.9 us
  Pallas kernels  47.8 us (98%)
  local copies, waits for them, and re-layouts  1.02 us (2%)
    pallas_call x1, Pallas kernels, body(): pl.pallas_call(kernel, name='cell', out_shape=pltpu.VMEM((seqs, span, 204...  47.8 us
    unnamed x1, local copies, waits for them, and re-layouts  1.02 us

profile of v3, /device:TPU:14, one launch (start us, length us, event | category | flops | bytes accessed | tf_op | source)
XLA Modules:
  0.0 48.9 jit_solution(6311028946287633405)
XLA Ops:
  0.0 47.8 %cell.1 = bf16[2,144,2048]{2,1,0:T(8,128)(2,1)S(1)} custom-call(bf16[16,144,128]{2,1,0:T(8,128)(2,1)} %bitcast.7, bf16[16,144,128]{2,1,0:T(8,128)(2,1)} %bitcast.8, bf16[16,144,128]{2,1,0:T(8,128)(2,1)} %bitcast.9, bf16[16,144]{1,0:T(8,128)(2,1)} %bitcast.12, bf16[16,144]{1,0:T(8,128)(2,1)} %bitcast.13, bf16[16,144,128]{2,1,0:T(8,128)(2,1)} %bitcast.10, ...), custom_call_target="tpu_custom_call" | custom-call | tf_op jit(solution)/shard_map/cell/pallas_call | solution.py:509
  47.9 1.0 %copy.10 = bf16[2,144,2048]{2,1,0:T(8,128)(2,1)} copy(bf16[2,144,2048]{2,1,0:T(8,128)(2,1)S(1)} %cell.1) | data formatting | bytes 2359296
